TPU v7x, 32 devices: a whole 2x2x4 slice. The times are simulated.
32 devices in a mesh: gr: 2 (over x), fs: 4 (over z), tp: 4 (over y, core).
Axes of the slice: x: 2, y: 2, z: 4, core: 2. Of those that a mesh axis runs over, the one named last changes fastest.
Arguments:
- tokens: bfloat16 [1536, 4096], P(('gr', 'fs'), 'tp'), may hold values from -6 to 6
- route_ids: int32 [1536, 2], P(('gr', 'fs')), may hold values from 0 to 3, all different within a row; in each aligned block of 192 rows (0 to 191, 192 to 383, ...) at most 192 rows name the same one
- route_logits: float32 [1536, 2], P(('gr', 'fs')), may hold values from -6 to 6
- gain: float32 [4096], P(('gr', 'fs')), may hold values from 0.1 to 1.9
- gate_master: float32 [4, 4096, 2048], P(None, ('gr', 'fs'), 'tp'), may hold values from -6 to 6
- up_master: float32 [4, 4096, 2048], P(None, ('gr', 'fs'), 'tp'), may hold values from -6 to 6
- down_master: float32 [4, 2048, 4096], P(None, ('gr', 'fs'), 'tp'), may hold values from -6 to 6
Outputs:
- gate_weight: bfloat16 [4, 4096, 2048], P('fs', None, 'tp')
- up_weight: bfloat16 [4, 4096, 2048], P('fs', None, 'tp')
- down_weight: bfloat16 [4, 2048, 4096], P('fs', 'tp')
- mixed_out: bfloat16 [1536, 4096], P(('gr', 'fs'), 'tp')
Inputs may be any that keep to these rules, and one draw needn't show every extreme that they name: `route_ids`: each row names 2 different experts; among the rows of one device no expert is named by more than 192 rows, a bound that some block reaches.
All inputs are finite; a program needn't handle non-finite values.
Results may differ from a plain program's by a relative error of at most 0.015.
Values may be sent and summed in bfloat16 or wider, within the bound.
A program may use at most 128 MiB of HBM per device.

v0:
```python
import jax
import jax.numpy as jnp
from jax import lax
from jax.sharding import PartitionSpec as P

EPS = 1e-06


def slot_tables(route_ids, experts, capacity):
    assign_count = route_ids.shape[0] * route_ids.shape[1]
    flattened = route_ids.reshape(assign_count)
    onehot = (flattened[:, None] == jnp.arange(experts, dtype=jnp.int32)[None, :]).astype(jnp.int32)
    earlier = jnp.cumsum(onehot, axis=0) - onehot
    slot_rank = jnp.sum(earlier * onehot, axis=1)
    position = flattened * capacity + slot_rank
    source = (
        jnp.full((experts * capacity,), assign_count, jnp.int32)
        .at[position]
        .set(jnp.arange(assign_count, dtype=jnp.int32))
    )
    return (position, source)


def fill_slots(normed, source, top_count, experts, capacity):
    token_total = normed.shape[0]
    padded = jnp.concatenate([normed, jnp.zeros((1, normed.shape[1]), normed.dtype)], axis=0)
    token_index = jnp.where(source < token_total * top_count, source // top_count, token_total)
    return padded[token_index].reshape(experts, capacity, normed.shape[1])


def body(tokens, route_ids, route_logits, gain, gate_master, up_master, down_master):
    experts = gate_master.shape[0]
    token_total = route_ids.shape[0]
    top_count = route_ids.shape[1]
    capacity = 2 * token_total * top_count // experts
    row_gain = gain[None, :, None]
    gate_cast = (gate_master * row_gain).astype(jnp.bfloat16)
    up_cast = (up_master * row_gain).astype(jnp.bfloat16)
    down_cast = down_master.astype(jnp.bfloat16)
    owner_gate, owner_up, owner_down = (
        lax.all_to_all(gate_cast, "fs", split_axis=0, concat_axis=1, tiled=True),
        lax.all_to_all(up_cast, "fs", split_axis=0, concat_axis=1, tiled=True),
        lax.all_to_all(down_cast, "fs", split_axis=0, concat_axis=1, tiled=True),
    )
    gate_full, up_full, down_full = (
        lax.all_gather(owner_gate, "gr", axis=1, tiled=True),
        lax.all_gather(owner_up, "gr", axis=1, tiled=True),
        lax.all_gather(owner_down, "gr", axis=1, tiled=True),
    )
    down_rows = lax.all_to_all(down_full, "tp", split_axis=1, concat_axis=2, tiled=True)
    sigmoid_vals = jax.nn.sigmoid(route_logits)
    shares = sigmoid_vals / jnp.sum(sigmoid_vals, axis=1, keepdims=True)
    position, source = slot_tables(route_ids, experts, capacity)
    model_width = gate_full.shape[1]
    full_rows = lax.all_gather(tokens, "tp", axis=1, tiled=True)
    float_rows = full_rows.astype(jnp.float32)
    normed = (
        float_rows * lax.rsqrt(jnp.mean(float_rows * float_rows, axis=1, keepdims=True) + EPS)
    ).astype(jnp.bfloat16)
    buffer = fill_slots(normed, source, top_count, experts, capacity)
    arrived = lax.all_to_all(buffer, "fs", split_axis=0, concat_axis=1, tiled=True)
    gate_sum = jnp.einsum("erd,edf->erf", arrived, gate_full, preferred_element_type=jnp.float32)
    up_sum = jnp.einsum("erd,edf->erf", arrived, up_full, preferred_element_type=jnp.float32)
    scale_in = model_width ** (-0.5)
    hidden = (jax.nn.silu(gate_sum * scale_in) * (up_sum * scale_in)).astype(jnp.bfloat16)
    partial_value = jnp.einsum(
        "erf,efd->erd", hidden, down_rows, preferred_element_type=jnp.float32
    )
    summed = lax.psum_scatter(
        partial_value.astype(jnp.bfloat16), "tp", scatter_dimension=2, tiled=True
    ).astype(jnp.float32)
    expert_out = (summed * down_full.shape[1] ** (-0.5)).astype(jnp.bfloat16)
    returned = lax.all_to_all(expert_out, "fs", split_axis=1, concat_axis=0, tiled=True)
    picked = returned.reshape(experts * capacity, returned.shape[2])[position].astype(jnp.float32)
    weighted = picked * shares.reshape(token_total * top_count)[:, None]
    mixed_out = jnp.sum(weighted.reshape(token_total, top_count, returned.shape[2]), axis=1).astype(
        jnp.bfloat16
    )
    return (gate_full, up_full, down_rows, mixed_out)


def solution(mesh):
    in_specs = (
        P(("gr", "fs"), "tp"),
        P(("gr", "fs"), None),
        P(("gr", "fs"), None),
        P(("gr", "fs")),
        P(None, ("gr", "fs"), "tp"),
        P(None, ("gr", "fs"), "tp"),
        P(None, ("gr", "fs"), "tp"),
    )
    out_specs = (
        P("fs", None, "tp"),
        P("fs", None, "tp"),
        P("fs", "tp", None),
        P(("gr", "fs"), "tp"),
    )
    return jax.shard_map(body, mesh=mesh, in_specs=in_specs, out_specs=out_specs, check_vma=False)
```

profile of v0, /device:TPU:0, one launch (start us, length us, event | category | flops | bytes accessed | tf_op | source)
XLA Modules:
  0.0 530.9 jit_solution(6687284316396528108)
XLA Ops:
  11.0 6.5 %all-to-all-start.2 = ((bf16[4,256,1024]{2,1,0:T(8,128)(2,1)}), bf16[4,256,1024]{2,1,0:T(8,128)(2,1)S(1)}, u32[]{:S(2)}, u32[]{:S(2)}) async-start(bf16[4,256,1024]{2,1,0:T(8,128)(2,1)} %convert_element_type.50), calls=%async_computation.2 | async-start | bytes 4194304 | tf_op jit(solution)/shard_map/all_to_all | solution.py:43
  17.5 6.8 %multiply_convert_fusion = (bf16[4,512,512]{2,1,0:T(8,128)(2,1)}, bf16[4,512,512]{2,1,0:T(8,128)(2,1)}) fusion(f32[4,512,512]{2,1,0:T(8,128)} %param.12, f32[512]{0:T(512)S(1)} %copy-done.5, f32[4,512,512]{2,1,0:T(8,128)} %param.11), kind=kLoop, calls=%fused_computation.9 | loop fusion | flops 4194304 | bytes 12584960 | tf_op jit(solution)/shard_map/convert_element_type | solution.py:38
  24.2 41.4 %all-to-all-done.2 = bf16[4,256,1024]{2,1,0:T(8,128)(2,1)S(1)} async-done(((bf16[4,256,1024]{2,1,0:T(8,128)(2,1)}), bf16[4,256,1024]{2,1,0:T(8,128)(2,1)S(1)}, u32[]{:S(2)}, u32[]{:S(2)}) %all-to-all-start.2) | async-done | bytes 2097184 | tf_op jit(solution)/shard_map/all_to_all | solution.py:43
  71.4 47.0 %all-to-all-done.1 = bf16[4,512,512]{2,1,0:T(8,128)(2,1)S(1)} async-done(((bf16[4,512,512]{2,1,0:T(8,128)(2,1)}), bf16[4,512,512]{2,1,0:T(8,128)(2,1)S(1)}, u32[]{:S(2)}, u32[]{:S(2)}) %all-to-all-start.1) | async-done | bytes 2097184 | tf_op jit(solution)/shard_map/all_to_all | solution.py:42
  123.6 8.2 %all-gather.9.cloned.1.call-done = bf16[1,2048,1024]{2,1,0:T(8,128)(2,1)} async-done(((bf16[1,1024,1024]{2,1,0:T(8,128)(2,1)}), bf16[1,2048,1024]{2,1,0:T(8,128)(2,1)}) %all-gather.9.cloned.1.call-update) | async-done | bytes 4194320 | tf_op jit(solution)/shard_map/all_gather | solution.py:48
  131.7 8.6 %copy.48 = bf16[1,2048,1024]{2,0,1:T(2,128)(2,1)} copy(bf16[1,2048,1024]{2,1,0:T(8,128)(2,1)} %all-gather.9.cloned.1.call-done) | data formatting | bytes 8388608 | tf_op jit(solution)/shard_map/all_gather | solution.py:48
  140.8 26.0 %reduce.4 = bf16[2048,1024]{1,0:T(8,128)(2,1)} reduce(bf16[2048,1,1024]{2,1,0:T(2,128)(2,1)} %bitcast.63, bf16[]{:T(256)} %broadcast.121), dimensions={1}, to_apply=%bitcast.59.reduce_sub_computation | reduce | bytes 8388610
  166.9 6.2 %reshape.164 = bf16[4,2,262144]{2,1,0:T(2,128)(2,1)} reshape(bf16[2048,1024]{1,0:T(8,128)(2,1)} %reduce.4) | data formatting | bytes 8388608
  173.1 5.0 all-to-all-start.3
  187.4 5.7 %gather_fusion = bf16[768,4096]{1,0:T(8,128)(2,1)} fusion(bf16[193,4096]{1,0:T(8,128)(2,1)S(1)} %concatenate.3, s32[1024]{0:T(1024)S(1)} %pad_clamp_fusion.1), kind=kCustom, calls=%fused_computation | custom fusion | bytes 12585984 | tf_op jit(solution)/shard_map/gather | solution.py:28
  193.1 33.3 %all-to-all-done.3 = bf16[4,2,262144]{2,1,0:T(2,128)(2,1)} async-done(((bf16[4,2,262144]{2,1,0:T(2,128)(2,1)}), bf16[4,2,262144]{2,1,0:T(2,128)(2,1)}, u32[]{:S(2)}, u32[]{:S(2)}) %all-to-all-start.3) | async-done | bytes 4194336 | tf_op jit(solution)/shard_map/all_to_all | solution.py:50
  226.3 5.3 %all-to-all-start.4 = ((bf16[4,192,4096]{2,1,0:T(8,128)(2,1)}), bf16[4,192,4096]{2,1,0:T(8,128)(2,1)}, u32[]{:S(2)}, u32[]{:S(2)}) async-start(bf16[4,192,4096]{2,1,0:T(8,128)(2,1)} %bitcast.65), calls=%async_computation.4 | async-start | bytes 12582912 | tf_op jit(solution)/shard_map/all_to_all | solution.py:61
  233.5 7.4 %reshape.165 = bf16[2048,1,1024]{2,1,0:T(2,128)(2,1)} reshape(bf16[4,2,262144]{2,1,0:T(2,128)(2,1)} %all-to-all-done.3) | data formatting | bytes 8388608
  240.9 7.9 %copy.40 = bf16[1,2048,1024]{2,1,0:T(8,128)(2,1)} copy(bf16[1,2048,1024]{2,0,1:T(2,128)(2,1)} %bitcast.64) | data formatting | bytes 8388608
  248.9 6.2 %copy.32 = bf16[1,512,4,1024]{1,3,2,0:T(8,128)(2,1)} copy(bf16[1,512,4,1024]{3,1,2,0:T(8,128)(2,1)} %bitcast.66) | data formatting | bytes 8388608 | tf_op jit(solution)/shard_map/all_to_all | solution.py:50
  255.1 35.2 %all-gather.7.cloned.1.call-done = bf16[1,4096,512]{2,1,0:T(8,128)(2,1)} async-done(((bf16[1,2048,512]{2,1,0:T(8,128)(2,1)}), bf16[1,4096,512]{2,1,0:T(8,128)(2,1)}) %all-gather.7.cloned.1.call-update) | async-done | bytes 4194320 | tf_op jit(solution)/shard_map/all_gather | solution.py:47
  290.3 79.5 %all-to-all-done.4 = bf16[4,192,4096]{2,1,0:T(8,128)(2,1)} async-done(((bf16[4,192,4096]{2,1,0:T(8,128)(2,1)}), bf16[4,192,4096]{2,1,0:T(8,128)(2,1)}, u32[]{:S(2)}, u32[]{:S(2)}) %all-to-all-start.4) | async-done | bytes 6291488 | tf_op jit(solution)/shard_map/all_to_all | solution.py:61
  369.8 6.7 %fusion.1 = f32[768,512]{1,0:T(8,128)S(1)} fusion(bf16[768,4096]{1,0:T(8,128)(2,1)} %bitcast.7, bf16[1,4096,512]{2,1,0:T(8,128)(2,1)} %all-gather.7.cloned.1.call-done), kind=kOutput, calls=%fused_computation.5 | convolution fusion | flops 3221225472 | bytes 12058624 | tf_op jit(solution)/shard_map/erd,edf->erf/dot_general | solution.py:63
  376.6 13.5 %fusion = bf16[1,768,4096]{2,1,0:T(8,128)(2,1)} fusion(bf16[512,4096]{0,1:T(8,128)(2,1)} %bitcast.67, f32[768,512]{1,0:T(8,128)S(1)} %fusion.1, bf16[768,4096]{1,0:T(8,128)(2,1)} %bitcast.7, bf16[1,4096,512]{2,1,0:T(8,128)(2,1)} %all-gather.5.cloned.1.call-done), kind=kOutput, calls=%fused_computation.4 | convolution fusion | flops 6448742400 | bytes 22544384 | tf_op jit(solution)/shard_map/erf,efd->erd/dot_general | solution.py:66
  390.1 55.4 %reduce-scatter.2.cloned.1.call-done = bf16[1,768,1024]{2,1,0:T(8,128)(2,1)} async-done(((bf16[1,768,4096]{2,1,0:T(8,128)(2,1)}), bf16[1,768,1024]{2,1,0:T(8,128)(2,1)}) %reduce-scatter.2.cloned.1.call-update) | async-done | bytes 1572880 | tf_op jit(solution)/shard_map/reduce_scatter | solution.py:69
  449.7 11.2 %reduce.5 = bf16[768,1024]{1,0:T(8,128)(2,1)} reduce(bf16[768,1,1024]{2,1,0:T(2,128)(2,1)S(1)} %bitcast.69, bf16[]{:T(256)} %broadcast.121), dimensions={1}, to_apply=%bitcast.60.reduce_sub_computation | reduce | bytes 3145730
  469.8 6.3 %copy.39 = bf16[1,512,4096]{2,1,0:T(8,128)(2,1)} copy(bf16[1,512,4096]{1,2,0:T(8,128)(2,1)} %bitcast.68) | data formatting | bytes 8388608
  476.2 30.3 %all-to-all-done.5 = bf16[4,2,98304]{2,1,0:T(2,128)(2,1)S(1)} async-done(((bf16[4,2,98304]{2,1,0:T(2,128)(2,1)}), bf16[4,2,98304]{2,1,0:T(2,128)(2,1)S(1)}, u32[]{:S(2)}, u32[]{:S(2)}) %all-to-all-start.5) | async-done | bytes 1572896 | tf_op jit(solution)/shard_map/all_to_all | solution.py:73
  517.5 4.6 copy.52
  (64 shorter events, 52.3 us)
Async XLA Ops:
  11.0 6.5 %copy-start.5 = (f32[512]{0:T(512)S(1)}, f32[512]{0:T(512)}, u32[]{:S(2)}) copy-start(f32[512]{0:T(512)} %param.10) | copy-start | bytes 6148
  11.0 54.7 %all-to-all-start.2 = ((bf16[4,256,1024]{2,1,0:T(8,128)(2,1)}), bf16[4,256,1024]{2,1,0:T(8,128)(2,1)S(1)}, u32[]{:S(2)}, u32[]{:S(2)}) async-start(bf16[4,256,1024]{2,1,0:T(8,128)(2,1)} %convert_element_type.50), calls=%async_computation.2 | async-start | bytes 4194304 | tf_op jit(solution)/shard_map/all_to_all | solution.py:43
  65.7 1.3 copy-start.1
  67.0 51.3 %all-to-all-start.1 = ((bf16[4,512,512]{2,1,0:T(8,128)(2,1)}), bf16[4,512,512]{2,1,0:T(8,128)(2,1)S(1)}, u32[]{:S(2)}, u32[]{:S(2)}) async-start(bf16[4,512,512]{2,1,0:T(8,128)(2,1)} %get-tuple-element.16), calls=%async_computation.1 | async-start | bytes 4194304 | tf_op jit(solution)/shard_map/all_to_all | solution.py:42
  70.6 61.1 %all-gather.9.cloned.1.call-start = ((), (), s32[]{:S(2)}) async-start(), calls=%async_computation.9 | async-start | bytes 6291456 | tf_op jit(solution)/shard_map/all_gather | solution.py:48
  118.3 22.0 %copy-start = (bf16[4,512,512]{2,1,0:T(8,128)(2,1)}, bf16[4,512,512]{2,1,0:T(8,128)(2,1)S(1)}, u32[]{:S(2)}) copy-start(bf16[4,512,512]{2,1,0:T(8,128)(2,1)S(1)} %all-to-all-done.1) | copy-start | bytes 6291460
  118.3 54.7 %all-to-all-start = ((bf16[4,512,512]{2,1,0:T(8,128)(2,1)}), bf16[4,512,512]{2,1,0:T(8,128)(2,1)}, u32[]{:S(2)}, u32[]{:S(2)}) async-start(bf16[4,512,512]{2,1,0:T(8,128)(2,1)} %get-tuple-element.17), calls=%async_computation | async-start | bytes 4194304 | tf_op jit(solution)/shard_map/all_to_all | solution.py:41
  122.8 60.8 %all-gather.11.cloned.1.call-start = ((), (), s32[]{:S(2)}) async-start(), calls=%async_computation.10 | async-start | bytes 1966080 | tf_op jit(solution)/shard_map/all_gather | solution.py:55
  173.1 5.1 copy-start.3
  173.1 53.3 %all-to-all-start.3 = ((bf16[4,2,262144]{2,1,0:T(2,128)(2,1)}), bf16[4,2,262144]{2,1,0:T(2,128)(2,1)}, u32[]{:S(2)}, u32[]{:S(2)}) async-start(bf16[4,2,262144]{2,1,0:T(2,128)(2,1)} %reshape.164), calls=%async_computation.3 | async-start | bytes 8388608 | tf_op jit(solution)/shard_map/all_to_all | solution.py:50
  226.3 143.4 %all-to-all-start.4 = ((bf16[4,192,4096]{2,1,0:T(8,128)(2,1)}), bf16[4,192,4096]{2,1,0:T(8,128)(2,1)}, u32[]{:S(2)}, u32[]{:S(2)}) async-start(bf16[4,192,4096]{2,1,0:T(8,128)(2,1)} %bitcast.65), calls=%async_computation.4 | async-start | bytes 12582912 | tf_op jit(solution)/shard_map/all_to_all | solution.py:61
  231.7 58.6 %all-gather.7.cloned.1.call-start = ((), (), s32[]{:S(2)}) async-start(), calls=%async_computation.8 | async-start | bytes 6291456 | tf_op jit(solution)/shard_map/all_gather | solution.py:47
  232.4 144.1 %all-gather.5.cloned.1.call-start = ((), (), s32[]{:S(2)}) async-start(), calls=%async_computation.7 | async-start | bytes 6291456 | tf_op jit(solution)/shard_map/all_gather | solution.py:46
  233.0 212.5 %reduce-scatter.2.cloned.1.call-start = ((), (), s32[]{:S(2)}) async-start(), calls=%async_computation.11 | async-start | bytes 7864320 | tf_op jit(solution)/shard_map/reduce_scatter | solution.py:69
  460.9 8.7 %copy-start.4 = (f32[192,2]{0,1:T(2,128)S(1)}, f32[192,2]{0,1:T(2,128)}, u32[]{:S(2)}) copy-start(f32[192,2]{0,1:T(2,128)} %param.9) | copy-start | bytes 4612
  465.1 41.4 %all-to-all-start.5 = ((bf16[4,2,98304]{2,1,0:T(2,128)(2,1)}), bf16[4,2,98304]{2,1,0:T(2,128)(2,1)S(1)}, u32[]{:S(2)}, u32[]{:S(2)}) async-start(bf16[4,2,98304]{2,1,0:T(2,128)(2,1)} %reshape.166), calls=%async_computation.6 | async-start | bytes 3145728 | tf_op jit(solution)/shard_map/all_to_all | solution.py:73
  517.5 4.6 copy-start.2
Sparse Core Ops, SparseCore 0:
  73.5 58.1 all-gather.8
  133.3 19.6 all-gather.10
  234.0 56.2 all-gather.6
  291.7 56.7 all-gather.4
  390.2 55.2 reduce-scatter.1
where the time goes:
time: 540 us; the launch traced here: 531 us
  waiting for transfers between devices  333 us (62%)
  local copies, waits for them, and re-layouts  75.8 us (14%)
  other arithmetic  57.6 us (11%)
  starting transfers between devices  30.2 us (6%)
  matrix products  20.2 us (4%)
  between operations  14.2 us (3%)
    all_to_all x1, waiting for transfers between devices, body(): lax.all_to_all(buffer, 'fs', split_axis=0, concat_axis=1, tiled=True)  79.5 us
    reduce_scatter x1, waiting for transfers between devices, body(): lax.psum_scatter(partial_value.astype(jnp.bfloat16), 'tp', scatter_dimens...  55.4 us
    all_to_all x1, waiting for transfers between devices, body(): lax.all_to_all(up_cast, 'fs', split_axis=0, concat_axis=1, tiled=True)  47 us
    unnamed x23, local copies, waits for them, and re-layouts  45.9 us
    all_to_all x1, waiting for transfers between devices, body(): lax.all_to_all(down_cast, 'fs', split_axis=0, concat_axis=1, tiled=True)  41.4 us
    unnamed x3, other arithmetic  37.3 us
    all_gather x1, waiting for transfers between devices, body(): lax.all_gather(owner_up, 'gr', axis=1, tiled=True)  35.2 us
    all_to_all x1, waiting for transfers between devices, body(): lax.all_to_all(down_full, 'tp', split_axis=1, concat_axis=2, tiled=True)  33.3 us
  transfers between devices with their start and end apart: 11, of which 8 were waited for; matrix products, arithmetic and copies ran while one was open for 18% of the time, Pallas kernels for 0%

commit v1 on v0

--- a/solution.py
+++ b/solution.py
@@ -4,6 +4,24 @@
 from jax.sharding import PartitionSpec as P
 
 EPS = 1e-06
+
+
+def write_turns_here(incoming_x, chip_axis):
+    out_arr = lax.axis_size(chip_axis)
+    y_new = lax.axis_index(chip_axis)
+    near, wide_out = (out_arr, y_new)
+    placed = incoming_x.shape[0] // near
+    top = jnp.roll(incoming_x, -wide_out * placed, axis=0)
+    work_now = lax.slice_in_dim(top, 0, placed, axis=0)
+    block_list = [work_now]
+    for hop_no in tuple(range(1, near)):
+        then = lax.slice_in_dim(top, hop_no * placed, (hop_no + 1) * placed, axis=0)
+        n_now = lax.ppermute(
+            then, axis_name=chip_axis, perm=[(dev, (dev + hop_no) % near) for dev in range(near)]
+        )
+        block_list.append(n_now)
+    w1 = jnp.concatenate(block_list[::-1], axis=1)
+    return jnp.roll(w1, (wide_out + 1) * block_list[0].shape[1], axis=1)
 
 
 def slot_tables(route_ids, experts, capacity):
@@ -39,7 +57,7 @@
     down_cast = down_master.astype(jnp.bfloat16)
     owner_gate, owner_up, owner_down = (
         lax.all_to_all(gate_cast, "fs", split_axis=0, concat_axis=1, tiled=True),
-        lax.all_to_all(up_cast, "fs", split_axis=0, concat_axis=1, tiled=True),
+        write_turns_here(up_cast, "fs"),
         lax.all_to_all(down_cast, "fs", split_axis=0, concat_axis=1, tiled=True),
     )
     gate_full, up_full, down_full = (

time: 540 us -> 628 us (1.16)
  blocking collectives: 0 us -> 54.4 us
  waiting for transfers between devices: 333 us -> 367 us
    ppermute x0 -> x3, waiting for transfers between devices: none -> 173 us  [write_turns_here(): lax.ppermute(then, axis_name=chip_axis, perm=[(dev, (dev + hop_no) % near...]
    all_to_all x2 -> x0, waiting for transfers between devices: 88.4 us -> none  [the longest x1 47 us: body(): lax.all_to_all(up_cast, 'fs', split_axis=0, concat_axis=1, tiled=True)]
    all_to_all x1, waiting for transfers between devices: 79.5 us -> 0.01 us  [body(): lax.all_to_all(buffer, 'fs', split_axis=0, concat_axis=1, tiled=True)]
    all_to_all x0 -> x1, blocking collectives: none -> 54.4 us  [body(): lax.all_to_all(down_cast, 'fs', split_axis=0, concat_axis=1, tiled=True)]
    all_gather x1, waiting for transfers between devices: 8.17 us -> 44.9 us  [body(): lax.all_gather(owner_down, 'gr', axis=1, tiled=True)]
    all_to_all x2 -> x0, starting transfers between devices: 10.1 us -> none  [the longest x1 6.48 us: body(): lax.all_to_all(down_cast, 'fs', split_axis=0, concat_axis=1, tiled=True)]
    all_gather x1, waiting for transfers between devices: 35.2 us -> 25.3 us  [body(): lax.all_gather(owner_up, 'gr', axis=1, tiled=True)]
    unnamed x23 -> x28, local copies, waits for them, and re-layouts: 45.9 us -> 48 us
  transfers between devices with their start and end apart: 11 -> 12, of which waited for: 8 -> 7; matrix products, arithmetic and copies ran while one was open for 18% -> 17% of each run, Pallas kernels for 0% -> 0%
where the time goes in v1:
time: 628 us; the launch traced here: 619 us
  waiting for transfers between devices  367 us (58%)
  local copies, waits for them, and re-layouts  80.6 us (13%)
  other arithmetic  58.6 us (9%)
  blocking collectives  54.4 us (9%)
  starting transfers between devices  24 us (4%)
  matrix products  20.2 us (3%)
  between operations  14.3 us (2%)
    ppermute x3, waiting for transfers between devices, write_turns_here(): lax.ppermute(then, axis_name=chip_axis, perm=[(dev, (dev + hop_no) % near...  173 us
    reduce_scatter x1, waiting for transfers between devices, body(): lax.psum_scatter(partial_value.astype(jnp.bfloat16), 'tp', scatter_dimens...  58.1 us
    all_to_all x1, blocking collectives, body(): lax.all_to_all(down_cast, 'fs', split_axis=0, concat_axis=1, tiled=True)  54.4 us
    unnamed x28, local copies, waits for them, and re-layouts  48 us
    all_gather x1, waiting for transfers between devices, body(): lax.all_gather(owner_down, 'gr', axis=1, tiled=True)  44.9 us
    unnamed x3, other arithmetic  37.3 us
    all_to_all x1, waiting for transfers between devices, body(): lax.all_to_all(down_full, 'tp', split_axis=1, concat_axis=2, tiled=True)  33.3 us
    all_to_all x1, waiting for transfers between devices, body(): lax.all_to_all(expert_out, 'fs', split_axis=1, concat_axis=0, tiled=True)  30.3 us
  transfers between devices with their start and end apart: 12, of which 7 were waited for; matrix products, arithmetic and copies ran while one was open for 17% of the time, Pallas kernels for 0%

profile of v1, /device:TPU:0, one launch (start us, length us, event | category | flops | bytes accessed | tf_op | source)
XLA Modules:
  0.0 618.8 jit_solution(10050213905173437280)
XLA Ops:
  9.7 54.4 %all_to_all.60 = bf16[4,256,1024]{2,1,0:T(8,128)(2,1)} all-to-all(bf16[4,256,1024]{2,1,0:T(8,128)(2,1)S(1)} %convert_element_type.50), channel_id=1, replica_groups=mesh['gr'=2,'fs'=4,'tp'=4] {'fs'}, dimensions={0} | all-to-all | bytes 4194304 | tf_op jit(solution)/shard_map/all_to_all | solution.py:61
  64.2 6.8 %multiply_convert_fusion = (bf16[4,512,512]{2,1,0:T(8,128)(2,1)}, bf16[4,512,512]{2,1,0:T(8,128)(2,1)}) fusion(f32[4,512,512]{2,1,0:T(8,128)} %param.12, f32[512]{0:T(512)S(1)} %copy-done.4, f32[4,512,512]{2,1,0:T(8,128)} %param.11), kind=kLoop, calls=%fused_computation.11 | loop fusion | flops 4194304 | bytes 12584960 | tf_op jit(solution)/shard_map/convert_element_type | solution.py:56
  75.4 44.9 %all-gather.9.cloned.1.call-done = bf16[1,2048,1024]{2,1,0:T(8,128)(2,1)} async-done(((bf16[1,1024,1024]{2,1,0:T(8,128)(2,1)}), bf16[1,2048,1024]{2,1,0:T(8,128)(2,1)}) %all-gather.9.cloned.1.call-update) | async-done | bytes 4194320 | tf_op jit(solution)/shard_map/all_gather | solution.py:66
  120.3 8.6 %copy.48 = bf16[1,2048,1024]{2,0,1:T(2,128)(2,1)} copy(bf16[1,2048,1024]{2,1,0:T(8,128)(2,1)} %all-gather.9.cloned.1.call-done) | data formatting | bytes 8388608 | tf_op jit(solution)/shard_map/all_gather | solution.py:66
  129.4 26.0 %reduce.4 = bf16[2048,1024]{1,0:T(8,128)(2,1)} reduce(bf16[2048,1,1024]{2,1,0:T(2,128)(2,1)} %bitcast.62, bf16[]{:T(256)} %broadcast.127), dimensions={1}, to_apply=%bitcast.58.reduce_sub_computation | reduce | bytes 8388610
  155.5 6.2 %reshape.161 = bf16[4,2,262144]{2,1,0:T(2,128)(2,1)} reshape(bf16[2048,1024]{1,0:T(8,128)(2,1)} %reduce.4) | data formatting | bytes 8388608
  163.0 4.9 all-to-all-start.2
  177.2 5.7 gather_fusion
  182.8 33.3 %all-to-all-done.2 = bf16[4,2,262144]{2,1,0:T(2,128)(2,1)} async-done(((bf16[4,2,262144]{2,1,0:T(2,128)(2,1)}), bf16[4,2,262144]{2,1,0:T(2,128)(2,1)}, u32[]{:S(2)}, u32[]{:S(2)}) %all-to-all-start.2) | async-done | bytes 4194336 | tf_op jit(solution)/shard_map/all_to_all | solution.py:68
  216.1 5.3 all-to-all-start.3
  231.1 104.2 %collective-permute-done = bf16[1,512,512]{2,1,0:T(8,128)(2,1)S(1)} collective-permute-done((bf16[1,512,512]{2,1,0:T(8,128)(2,1)}, bf16[1,512,512]{2,1,0:T(8,128)(2,1)S(1)}, u32[]{:S(2)}, u32[]{:S(2)}) %collective-permute-start) | collective-permute-done | bytes 524320 | tf_op jit(solution)/shard_map/ppermute | solution.py:19
  335.3 69.2 %collective-permute-done.1 = bf16[1,512,512]{2,1,0:T(8,128)(2,1)S(1)} collective-permute-done((bf16[1,512,512]{2,1,0:T(8,128)(2,1)}, bf16[1,512,512]{2,1,0:T(8,128)(2,1)S(1)}, u32[]{:S(2)}, u32[]{:S(2)}) %collective-permute-start.1) | collective-permute-done | bytes 524320 | tf_op jit(solution)/shard_map/ppermute | solution.py:19
  408.3 7.7 %reshape.162 = bf16[2048,1,1024]{2,1,0:T(2,128)(2,1)} reshape(bf16[4,2,262144]{2,1,0:T(2,128)(2,1)} %all-to-all-done.2) | data formatting | bytes 8388608
  416.0 7.5 %copy.40 = bf16[1,2048,1024]{2,1,0:T(8,128)(2,1)} copy(bf16[1,2048,1024]{2,0,1:T(2,128)(2,1)} %bitcast.63) | data formatting | bytes 8388608
  423.5 6.2 copy.32
  429.7 6.7 %fusion.3 = f32[768,512]{1,0:T(8,128)S(1)} fusion(bf16[768,4096]{1,0:T(8,128)(2,1)} %bitcast.6, bf16[1,4096,512]{2,1,0:T(8,128)(2,1)} %all-gather.5.cloned.1.call-done), kind=kOutput, calls=%fused_computation.9 | convolution fusion | flops 3221225472 | bytes 12058624 | tf_op jit(solution)/shard_map/erd,edf->erf/dot_general | solution.py:80
  436.5 25.3 %all-gather.7.cloned.1.call-done = bf16[1,4096,512]{2,1,0:T(8,128)(2,1)} async-done(((bf16[1,2048,512]{2,1,0:T(8,128)(2,1)}), bf16[1,4096,512]{2,1,0:T(8,128)(2,1)}) %all-gather.7.cloned.1.call-update) | async-done | bytes 4194320 | tf_op jit(solution)/shard_map/all_gather | solution.py:65
  461.7 13.5 %fusion = bf16[1,768,4096]{2,1,0:T(8,128)(2,1)} fusion(bf16[512,4096]{0,1:T(8,128)(2,1)} %bitcast.66, f32[768,512]{1,0:T(8,128)S(1)} %fusion.3, bf16[768,4096]{1,0:T(8,128)(2,1)} %bitcast.6, bf16[1,4096,512]{2,1,0:T(8,128)(2,1)} %all-gather.7.cloned.1.call-done), kind=kOutput, calls=%fused_computation.4 | convolution fusion | flops 6448742400 | bytes 22544384 | tf_op jit(solution)/shard_map/erf,efd->erd/dot_general | solution.py:84
  475.2 58.1 %reduce-scatter.2.cloned.1.call-done = bf16[1,768,1024]{2,1,0:T(8,128)(2,1)} async-done(((bf16[1,768,4096]{2,1,0:T(8,128)(2,1)}), bf16[1,768,1024]{2,1,0:T(8,128)(2,1)}) %reduce-scatter.2.cloned.1.call-update) | async-done | bytes 1572880 | tf_op jit(solution)/shard_map/reduce_scatter | solution.py:87
  537.6 11.2 %reduce.5 = bf16[768,1024]{1,0:T(8,128)(2,1)} reduce(bf16[768,1,1024]{2,1,0:T(2,128)(2,1)S(1)} %bitcast.68, bf16[]{:T(256)} %broadcast.127), dimensions={1}, to_apply=%bitcast.59.reduce_sub_computation | reduce | bytes 3145730
  552.9 4.6 all-to-all-start.4
  557.7 6.3 %copy.39 = bf16[1,512,4096]{2,1,0:T(8,128)(2,1)} copy(bf16[1,512,4096]{1,2,0:T(8,128)(2,1)} %bitcast.67) | data formatting | bytes 8388608
  564.0 30.3 %all-to-all-done.4 = bf16[4,2,98304]{2,1,0:T(2,128)(2,1)S(1)} async-done(((bf16[4,2,98304]{2,1,0:T(2,128)(2,1)}), bf16[4,2,98304]{2,1,0:T(2,128)(2,1)S(1)}, u32[]{:S(2)}, u32[]{:S(2)}) %all-to-all-start.4) | async-done | bytes 1572896 | tf_op jit(solution)/shard_map/all_to_all | solution.py:91
  605.3 4.6 copy.59
  (76 shorter events, 53.0 us)
Async XLA Ops:
  7.2 113.2 %all-gather.9.cloned.1.call-start = ((), (), s32[]{:S(2)}) async-start(), calls=%async_computation.8 | async-start | bytes 6291456 | tf_op jit(solution)/shard_map/all_gather | solution.py:66
  9.7 54.5 %copy-start.4 = (f32[512]{0:T(512)S(1)}, f32[512]{0:T(512)}, u32[]{:S(2)}) copy-start(f32[512]{0:T(512)} %param.10) | copy-start | bytes 6148
  71.0 90.7 %all-to-all-start = ((bf16[4,512,512]{2,1,0:T(8,128)(2,1)}), bf16[4,512,512]{2,1,0:T(8,128)(2,1)S(1)}, u32[]{:S(2)}, u32[]{:S(2)}) async-start(bf16[4,512,512]{2,1,0:T(8,128)(2,1)} %get-tuple-element.20), calls=%async_computation | async-start | bytes 4194304 | tf_op jit(solution)/shard_map/all_to_all | solution.py:59
  74.7 98.7 %all-gather.11.cloned.1.call-start = ((), (), s32[]{:S(2)}) async-start(), calls=%async_computation.9 | async-start | bytes 1966080 | tf_op jit(solution)/shard_map/all_gather | solution.py:73
  161.7 6.2 %copy-start.2 = (s32[192,2]{0,1:T(2,128)S(1)}, s32[192,2]{0,1:T(2,128)}, u32[]{:S(2)}) copy-start(s32[192,2]{0,1:T(2,128)} %param.8) | copy-start | bytes 4612
  161.7 1.3 copy-start
  163.0 53.1 %all-to-all-start.2 = ((bf16[4,2,262144]{2,1,0:T(2,128)(2,1)}), bf16[4,2,262144]{2,1,0:T(2,128)(2,1)}, u32[]{:S(2)}, u32[]{:S(2)}) async-start(bf16[4,2,262144]{2,1,0:T(2,128)(2,1)} %reshape.161), calls=%async_computation.2 | async-start | bytes 8388608 | tf_op jit(solution)/shard_map/all_to_all | solution.py:68
  216.1 213.6 %all-to-all-start.3 = ((bf16[4,192,4096]{2,1,0:T(8,128)(2,1)}), bf16[4,192,4096]{2,1,0:T(8,128)(2,1)}, u32[]{:S(2)}, u32[]{:S(2)}) async-start(bf16[4,192,4096]{2,1,0:T(8,128)(2,1)} %bitcast.64), calls=%async_computation.3 | async-start | bytes 12582912 | tf_op jit(solution)/shard_map/all_to_all | solution.py:79
  221.5 208.3 %all-gather.5.cloned.1.call-start = ((), (), s32[]{:S(2)}) async-start(), calls=%async_computation.6 | async-start | bytes 6291456 | tf_op jit(solution)/shard_map/all_gather | solution.py:64
  222.2 239.5 %all-gather.7.cloned.1.call-start = ((), (), s32[]{:S(2)}) async-start(), calls=%async_computation.7 | async-start | bytes 6291456 | tf_op jit(solution)/shard_map/all_gather | solution.py:65
  225.8 109.4 %collective-permute-start = (bf16[1,512,512]{2,1,0:T(8,128)(2,1)}, bf16[1,512,512]{2,1,0:T(8,128)(2,1)S(1)}, u32[]{:S(2)}, u32[]{:S(2)}) collective-permute-start(bf16[1,512,512]{2,1,0:T(8,128)(2,1)} %get-tuple-element.18), channel_id=1, source_target_pairs={{0,12},{4,0},{8,4},{12,8},{1,13},{5,1},{9,5},{13,9},{2,14},{6,2},{... | collective-permute-start | bytes 1572872 | tf_op jit(solution)/shard_map/ppermute | solution.py:19
  229.5 174.9 %collective-permute-start.1 = (bf16[1,512,512]{2,1,0:T(8,128)(2,1)}, bf16[1,512,512]{2,1,0:T(8,128)(2,1)S(1)}, u32[]{:S(2)}, u32[]{:S(2)}) collective-permute-start(bf16[1,512,512]{2,1,0:T(8,128)(2,1)} %get-tuple-element.17), channel_id=1, source_target_pairs={{0,8},{4,12},{8,0},{12,4},{1,9},{5,13},{9,1},{13,5},{2,10},{6,14},... | collective-permute-start | bytes 1572872 | tf_op jit(solution)/shard_map/ppermute | solution.py:19
  229.5 174.9 %collective-permute-start.2 = (bf16[1,512,512]{2,1,0:T(8,128)(2,1)}, bf16[1,512,512]{2,1,0:T(8,128)(2,1)}, u32[]{:S(2)}, u32[]{:S(2)}) collective-permute-start(bf16[1,512,512]{2,1,0:T(8,128)(2,1)} %get-tuple-element.16), channel_id=1, source_target_pairs={{0,4},{4,8},{8,12},{12,0},{1,5},{5,9},{9,13},{13,1},{2,6},{6,10},{... | collective-permute-start | bytes 1572872 | tf_op jit(solution)/shard_map/ppermute | solution.py:19
  408.3 125.0 %reduce-scatter.2.cloned.1.call-start = ((), (), s32[]{:S(2)}) async-start(), calls=%async_computation.10 | async-start | bytes 7864320 | tf_op jit(solution)/shard_map/reduce_scatter | solution.py:87
  548.8 8.7 %copy-start.3 = (f32[192,2]{0,1:T(2,128)S(1)}, f32[192,2]{0,1:T(2,128)}, u32[]{:S(2)}) copy-start(f32[192,2]{0,1:T(2,128)} %param.9) | copy-start | bytes 4612
  552.9 41.4 %all-to-all-start.4 = ((bf16[4,2,98304]{2,1,0:T(2,128)(2,1)}), bf16[4,2,98304]{2,1,0:T(2,128)(2,1)S(1)}, u32[]{:S(2)}, u32[]{:S(2)}) async-start(bf16[4,2,98304]{2,1,0:T(2,128)(2,1)} %reshape.163), calls=%async_computation.5 | async-start | bytes 3145728 | tf_op jit(solution)/shard_map/all_to_all | solution.py:91
  605.3 4.6 copy-start.1
Sparse Core Ops, SparseCore 0:
  64.3 55.9 all-gather.8
  121.9 19.6 all-gather.10
  223.8 56.2 all-gather.4
  408.4 53.2 all-gather.6
  475.4 57.9 reduce-scatter.1
